TPU v7x, 128 devices: a whole 4x4x4 slice. The times are simulated.
128 devices in a mesh: sp: 16 (over z, y), tp: 8 (over x, core).
Axes of the slice: x: 4, y: 4, z: 4, core: 2. Of those that a mesh axis runs over, the one named last changes fastest.
Arguments:
- residual_in: bfloat16 [12288, 2048], P('sp', 'tp'), may hold values from -11 to 11
- queries: bfloat16 [12288, 1024], P('sp', 'tp'), may hold values from -6 to 6
- keys: bfloat16 [12288, 256], P('sp'), may hold values from -6 to 6
- values: bfloat16 [12288, 256], P('sp'), may hold values from -6 to 6
- query_gain: float32 [128], replicated, may hold values from 1.5 to 5
- key_norm_gain: float32 [128], replicated, may hold values from 1.5 to 5
- out_weight: bfloat16 [1024, 2048], P('tp'), may hold values from -0.1875 to 0.1875
- mlp_gain: float32 [2048], replicated, may hold values from 0.1 to 1.9
- gate_weight: bfloat16 [2048, 5632], P('sp', 'tp'), may hold values from -0.125 to 0.125
- up_weight: bfloat16 [2048, 5632], P('sp', 'tp'), may hold values from -0.125 to 0.125
- down_weight: bfloat16 [5632, 2048], P('tp', 'sp'), may hold values from -0.15625 to 0.15625
Outputs:
- layer_out: bfloat16 [12288, 2048], P('sp', 'tp')
All inputs are finite; a program needn't handle non-finite values.
Results may differ from a plain program's by a relative error of at most 0.012.
The roundings to bfloat16 on the way count: a program that leaves them out, or rounds other values in their place, can miss the bound.
Values may be sent and summed in bfloat16 or wider, within the bound.
A program may use at most 64 MiB of HBM per device.

v0:
```python
import jax
import jax.numpy as jnp
from jax import lax
from jax.sharding import PartitionSpec as P

D = 2048
HEAD_SIZE = 128
QUERY_HEADS = 8
KEY_VALUE_HEADS = 2
GRID = 64
eps = 1e-06
rotary_base = 10000.0


def sent_together(arrays, axis, dim, along):
    ends, at = ([], 0)
    for a in arrays[:-1]:
        at += a.shape[along]
        ends.append(at)
    both = jnp.concatenate(arrays, axis=along)
    return tuple(jnp.split(lax.all_gather(both, axis, axis=dim, tiled=True), ends, axis=along))


def laid_out(tiles, dim):
    tiles = jnp.moveaxis(tiles, 0, dim)
    lengths = tiles.shape
    return tiles.reshape(*lengths[:dim], lengths[dim] * lengths[dim + 1], *lengths[dim + 2 :])


def sent_to_all(x, axis):
    size = lax.axis_size(axis)
    return lax.all_to_all(jnp.broadcast_to(x[None], (size, *x.shape)), axis, 0, 0, tiled=True)


def gathered_copies(x, axis, dim):
    return laid_out(sent_to_all(x, axis), dim)


def taken_together(x, axis):
    everything = sent_to_all(x, axis)
    return jnp.sum(everything, axis=0)


def in_blocks(x, dim, size):
    lengths = x.shape
    tiles = x.reshape(*lengths[:dim], size, lengths[dim] // size, *lengths[dim + 1 :])
    return jnp.moveaxis(tiles, dim, 0)


def summed_on_arrival(x, axis, dim):
    tiles = in_blocks(x, dim, lax.axis_size(axis))
    arrived = lax.all_to_all(tiles, axis, split_axis=0, concat_axis=0, tiled=True)
    return arrived.astype(jnp.float32).sum(axis=0)


def apply_rotary(vectors, grid_positions):
    half_size = vectors.shape[-1] // 2
    frequency = rotary_base ** (-jnp.arange(0, half_size, 2, dtype=jnp.float32) / half_size)
    grid_row = (grid_positions // GRID).astype(jnp.float32)
    grid_col = (grid_positions % GRID).astype(jnp.float32)
    angles = jnp.concatenate(
        [grid_row[:, None] * frequency, grid_col[:, None] * frequency], axis=-1
    )[:, None, :]
    cosine_table = jnp.cos(angles)
    sine_table = jnp.sin(angles)
    first_half = vectors[..., :half_size]
    second_half = vectors[..., half_size:]
    return jnp.concatenate(
        [
            first_half * cosine_table - second_half * sine_table,
            first_half * sine_table + second_half * cosine_table,
        ],
        axis=-1,
    )


def per_head_norm(vectors, gain):
    return vectors * lax.rsqrt(jnp.mean(vectors * vectors, axis=-1, keepdims=True) + eps) * gain


def on_device(
    residual_in,
    queries,
    keys,
    values,
    query_gain,
    key_norm_gain,
    out_weight,
    mlp_gain,
    gate_weight,
    up_weight,
    down_weight,
):
    local_rows = residual_in.shape[0]
    local_heads = queries.shape[1] // HEAD_SIZE
    queries_per_group = QUERY_HEADS // KEY_VALUE_HEADS
    tp_index = lax.axis_index("tp")
    tp_count = lax.axis_size("tp")
    grid_positions = lax.axis_index("sp") * local_rows + jnp.arange(local_rows, dtype=jnp.int32)
    weight_cols = lax.all_to_all(out_weight, "tp", split_axis=1, concat_axis=0, tiled=True)
    query_rows = apply_rotary(
        per_head_norm(
            queries.astype(jnp.float32).reshape(local_rows, local_heads, HEAD_SIZE), query_gain
        ),
        grid_positions,
    ).astype(jnp.bfloat16)
    query_matrix = jnp.transpose(query_rows, (1, 0, 2)).reshape(local_heads * local_rows, HEAD_SIZE)
    shared = tp_index * local_heads // queries_per_group
    own_keys = lax.dynamic_slice_in_dim(keys, shared * HEAD_SIZE, HEAD_SIZE, 1)
    own_values = lax.dynamic_slice_in_dim(values, shared * HEAD_SIZE, HEAD_SIZE, 1)
    key_matrix = apply_rotary(
        per_head_norm(own_keys.astype(jnp.float32)[:, None, :], key_norm_gain), grid_positions
    )[:, 0, :].astype(jnp.bfloat16)
    score_scale = HEAD_SIZE ** (-0.5)
    query_count = local_heads * local_rows
    start_state = (
        jnp.full((query_count,), -1e30, jnp.float32),
        jnp.zeros((query_count,), jnp.float32),
        jnp.zeros((query_count, HEAD_SIZE), jnp.float32),
    )
    key_piece, value_piece = sent_together((key_matrix, own_values), "sp", 0, 1)
    piece_rows = key_piece.shape[0]
    block_count = -(-piece_rows // 2048)
    while piece_rows % block_count:
        block_count += 1
    block_width = piece_rows // block_count

    def one_block(block_index, state_inner):
        running_max, running_sum, weighted = state_inner
        block_keys = lax.dynamic_slice_in_dim(key_piece, block_index * block_width, block_width, 0)
        block_values = lax.dynamic_slice_in_dim(
            value_piece, block_index * block_width, block_width, 0
        )
        scores = (
            jnp.dot(query_matrix, block_keys.T, preferred_element_type=jnp.float32) * score_scale
        )
        new_max = jnp.maximum(running_max, jnp.max(scores, axis=1))
        factor = jnp.exp(running_max - new_max)
        weights = jnp.exp(scores - new_max[:, None])
        running_sum = running_sum * factor + jnp.sum(weights, axis=1)
        weighted = weighted * factor[:, None] + jnp.dot(
            weights.astype(jnp.bfloat16), block_values, preferred_element_type=jnp.float32
        )
        return (new_max, running_sum, weighted)

    running_max, running_sum, weighted = lax.fori_loop(0, block_count, one_block, start_state)
    attended = (weighted / running_sum[:, None]).astype(jnp.bfloat16)
    attended = jnp.transpose(
        attended.reshape(local_heads, local_rows, HEAD_SIZE), (1, 0, 2)
    ).reshape(local_rows, local_heads * HEAD_SIZE)
    own_width = residual_in.shape[1]
    attended_full = gathered_copies(attended, "tp", 1)
    group_width = local_heads * HEAD_SIZE
    share = jnp.zeros((local_rows, own_width), jnp.float32)
    for group_index in range(tp_count):
        left_part = attended_full[:, group_index * group_width : (group_index + 1) * group_width]
        right_part = weight_cols[group_index * group_width : (group_index + 1) * group_width, :]
        term = jnp.dot(left_part, right_part, preferred_element_type=jnp.float32).astype(
            jnp.bfloat16
        )
        share = share + term.astype(jnp.float32)
    residual_mid = residual_in.astype(jnp.float32) + share
    squares = taken_together(jnp.sum(residual_mid * residual_mid, axis=1), "tp")
    gain_own = lax.dynamic_slice_in_dim(mlp_gain, tp_index * own_width, own_width, 0)
    normed_own = (residual_mid * lax.rsqrt(squares / D + eps)[:, None] * gain_own).astype(
        jnp.bfloat16
    )
    normed = lax.all_gather(normed_own, "tp", axis=1, tiled=True)
    pieces = sent_together((gate_weight, up_weight), "sp", 0, 1)
    gate_out = jnp.dot(normed, pieces[0], preferred_element_type=jnp.float32)
    up_out = jnp.dot(normed, pieces[1], preferred_element_type=jnp.float32)
    hidden = (jax.nn.silu(gate_out) * up_out).astype(jnp.bfloat16)
    down_terms = jnp.dot(
        hidden,
        lax.all_gather(down_weight, "sp", axis=1, tiled=True),
        preferred_element_type=jnp.float32,
    )
    down_share = summed_on_arrival(down_terms.astype(jnp.bfloat16), "tp", 1)
    return (residual_mid + 0.5 * down_share).astype(jnp.bfloat16)


def solution(mesh):
    in_specs = (
        P("sp", "tp"),
        P("sp", "tp"),
        P("sp", None),
        P("sp", None),
        P(),
        P(),
        P("tp", None),
        P(),
        P("sp", "tp"),
        P("sp", "tp"),
        P("tp", "sp"),
    )
    out_specs = P("sp", "tp")
    return jax.shard_map(
        on_device, mesh=mesh, in_specs=in_specs, out_specs=out_specs, check_vma=False
    )
```

profile of v0, /device:TPU:1, one launch (start us, length us, event | category | flops | bytes accessed | tf_op | source)
XLA Modules:
  0.0 336.8 jit_solution(7837900333065985362)
XLA Ops:
  6.6 1.1 fusion.38
  7.7 1.1 fusion.41
  8.9 0.3 multiply_bitcast_fusion.1
  9.2 1.3 fusion.40
  10.5 1.8 fusion.44
  12.3 0.3 subtract_convert_fusion.1
  12.8 0.8 pad_maximum_fusion.1
  13.6 1.0 copy.61
  14.6 5.8 %all-to-all-start.1 = ((bf16[128,8,256]{0,2,1:T(8,128)(2,1)}), bf16[128,8,256]{0,2,1:T(8,128)(2,1)S(1)}, u32[]{:S(2)}, u32[]{:S(2)}) async-start(bf16[128,8,256]{0,2,1:T(8,128)(2,1)} %bitcast.9), calls=%async_computation.1 | async-start | bytes 1048576 | tf_op jit(solution)/shard_map/all_to_all | solution.py:100
  20.4 0.8 pad_maximum_fusion.2
  21.4 56.8 %all-gather.5.cloned.1.call-done = bf16[12288,256]{1,0:T(8,128)(2,1)} async-done(((bf16[768,256]{1,0:T(8,128)(2,1)}), bf16[12288,256]{1,0:T(8,128)(2,1)}) %all-gather.5.cloned.1.call-update) | async-done | bytes 6291472 | tf_op jit(solution)/shard_map/all_gather | solution.py:21
  78.2 4.7 %fusion.66 = (bf16[12288,128]{1,0:T(8,128)(2,1)}, bf16[12288,128]{1,0:T(8,128)(2,1)}) fusion(bf16[12288,256]{1,0:T(8,128)(2,1)} %all-gather.5.cloned.1.call-done), kind=kLoop, calls=%fused_computation.114 | loop fusion | bytes 12582912 | tf_op jit(solution)/shard_map/split | solution.py:21
  82.9 71.6 %while.18 = (s32[]{:T(128)}, f32[768]{0:T(1024)S(1)}, f32[768]{0:T(1024)S(1)}, f32[768,128]{1,0:T(8,128)S(1)}, bf16[12288,128]{1,0:T(8,128)(2,1)}, /*index=5*/bf...) while((s32[]{:T(128)}, f32[768]{0:T(1024)S(1)}, ...), condition=%wide.region_5.6_spmd.clone, body=%wide.region_2.5_spmd.clone.sunk | while | flops 818188032 | bytes 46121160 | solution.py:146
  82.9 4.7 %multiply_reduce_fusion.3 = (f32[768]{0:T(1024)S(1)}, f32[2048,768]{1,0:T(8,128)}) fusion(bf16[768,128]{1,0:T(8,128)(2,1)S(1)} %get-tuple-element.268, bf16[12288,128]{1,0:T(8,128)(2,1)} %get-tuple-element.267, s32[]{:T(128)S(6)} %select_n.55), kind=kOutput, calls=%fused_computation.1.clone.1 | convolution fusion | flops 405798144 | bytes 7015428 | tf_op jit(solution)/shard_map/while/body/eval_jaxpr/dot_general | solution.py:135
  87.6 4.2 %fusion.80 = f32[768]{0:T(1024)S(1)} fusion(f32[2048,768]{1,0:T(8,128)} %get-tuple-element.238, f32[768]{0:T(1024)S(1)} %select_maximum_fusion.2), kind=kLoop, calls=%fused_computation.3.clone.1 | loop fusion | flops 4717824 | bytes 6297600 | tf_op jit(solution)/shard_map/while/body/eval_jaxpr/reduce_sum | solution.py:140
  91.8 0.8 copy-done.1
  92.6 2.4 fusion.82
  95.0 4.7 %multiply_reduce_fusion.3 = (f32[768]{0:T(1024)S(1)}, f32[2048,768]{1,0:T(8,128)}) fusion(bf16[768,128]{1,0:T(8,128)(2,1)S(1)} %get-tuple-element.268, bf16[12288,128]{1,0:T(8,128)(2,1)} %get-tuple-element.267, s32[]{:T(128)S(6)} %select_n.55), kind=kOutput, calls=%fused_computation.1.clone.1 | convolution fusion | flops 405798144 | bytes 7015428 | tf_op jit(solution)/shard_map/while/body/eval_jaxpr/dot_general | solution.py:135
  99.6 4.1 %fusion.80 = f32[768]{0:T(1024)S(1)} fusion(f32[2048,768]{1,0:T(8,128)} %get-tuple-element.238, f32[768]{0:T(1024)S(1)} %select_maximum_fusion.2), kind=kLoop, calls=%fused_computation.3.clone.1 | loop fusion | flops 4717824 | bytes 6297600 | tf_op jit(solution)/shard_map/while/body/eval_jaxpr/reduce_sum | solution.py:140
  103.7 0.6 copy-done.1
  104.3 2.4 fusion.82
  106.7 4.7 %multiply_reduce_fusion.3 = (f32[768]{0:T(1024)S(1)}, f32[2048,768]{1,0:T(8,128)}) fusion(bf16[768,128]{1,0:T(8,128)(2,1)S(1)} %get-tuple-element.268, bf16[12288,128]{1,0:T(8,128)(2,1)} %get-tuple-element.267, s32[]{:T(128)S(6)} %select_n.55), kind=kOutput, calls=%fused_computation.1.clone.1 | convolution fusion | flops 405798144 | bytes 7015428 | tf_op jit(solution)/shard_map/while/body/eval_jaxpr/dot_general | solution.py:135
  111.4 4.2 %fusion.80 = f32[768]{0:T(1024)S(1)} fusion(f32[2048,768]{1,0:T(8,128)} %get-tuple-element.238, f32[768]{0:T(1024)S(1)} %select_maximum_fusion.2), kind=kLoop, calls=%fused_computation.3.clone.1 | loop fusion | flops 4717824 | bytes 6297600 | tf_op jit(solution)/shard_map/while/body/eval_jaxpr/reduce_sum | solution.py:140
  115.6 0.8 copy-done.1
  116.4 2.4 fusion.82
  118.8 4.7 %multiply_reduce_fusion.3 = (f32[768]{0:T(1024)S(1)}, f32[2048,768]{1,0:T(8,128)}) fusion(bf16[768,128]{1,0:T(8,128)(2,1)S(1)} %get-tuple-element.268, bf16[12288,128]{1,0:T(8,128)(2,1)} %get-tuple-element.267, s32[]{:T(128)S(6)} %select_n.55), kind=kOutput, calls=%fused_computation.1.clone.1 | convolution fusion | flops 405798144 | bytes 7015428 | tf_op jit(solution)/shard_map/while/body/eval_jaxpr/dot_general | solution.py:135
  123.5 4.2 %fusion.80 = f32[768]{0:T(1024)S(1)} fusion(f32[2048,768]{1,0:T(8,128)} %get-tuple-element.238, f32[768]{0:T(1024)S(1)} %select_maximum_fusion.2), kind=kLoop, calls=%fused_computation.3.clone.1 | loop fusion | flops 4717824 | bytes 6297600 | tf_op jit(solution)/shard_map/while/body/eval_jaxpr/reduce_sum | solution.py:140
  127.7 0.8 copy-done.1
  128.5 2.4 fusion.82
  130.9 4.7 %multiply_reduce_fusion.3 = (f32[768]{0:T(1024)S(1)}, f32[2048,768]{1,0:T(8,128)}) fusion(bf16[768,128]{1,0:T(8,128)(2,1)S(1)} %get-tuple-element.268, bf16[12288,128]{1,0:T(8,128)(2,1)} %get-tuple-element.267, s32[]{:T(128)S(6)} %select_n.55), kind=kOutput, calls=%fused_computation.1.clone.1 | convolution fusion | flops 405798144 | bytes 7015428 | tf_op jit(solution)/shard_map/while/body/eval_jaxpr/dot_general | solution.py:135
  135.6 4.2 %fusion.80 = f32[768]{0:T(1024)S(1)} fusion(f32[2048,768]{1,0:T(8,128)} %get-tuple-element.238, f32[768]{0:T(1024)S(1)} %select_maximum_fusion.2), kind=kLoop, calls=%fused_computation.3.clone.1 | loop fusion | flops 4717824 | bytes 6297600 | tf_op jit(solution)/shard_map/while/body/eval_jaxpr/reduce_sum | solution.py:140
  139.8 0.7 copy-done.1
  140.5 2.4 fusion.82
  142.9 4.7 %multiply_reduce_fusion.3 = (f32[768]{0:T(1024)S(1)}, f32[2048,768]{1,0:T(8,128)}) fusion(bf16[768,128]{1,0:T(8,128)(2,1)S(1)} %get-tuple-element.268, bf16[12288,128]{1,0:T(8,128)(2,1)} %get-tuple-element.267, s32[]{:T(128)S(6)} %select_n.55), kind=kOutput, calls=%fused_computation.1.clone.1 | convolution fusion | flops 405798144 | bytes 7015428 | tf_op jit(solution)/shard_map/while/body/eval_jaxpr/dot_general | solution.py:135
  147.5 4.0 %fusion.80 = f32[768]{0:T(1024)S(1)} fusion(f32[2048,768]{1,0:T(8,128)} %get-tuple-element.238, f32[768]{0:T(1024)S(1)} %select_maximum_fusion.2), kind=kLoop, calls=%fused_computation.3.clone.1 | loop fusion | flops 4717824 | bytes 6297600 | tf_op jit(solution)/shard_map/while/body/eval_jaxpr/reduce_sum | solution.py:140
  151.6 0.6 copy-done.1
  152.1 2.4 fusion.82
  154.9 1.3 broadcast_in_dim.17
  156.2 5.2 %all-to-all-start = ((bf16[8,768,128]{1,2,0:T(8,128)(2,1)}), bf16[8,768,128]{1,2,0:T(8,128)(2,1)S(1)}, u32[]{:S(2)}, u32[]{:S(2)}) async-start(bf16[8,768,128]{1,2,0:T(8,128)(2,1)} %broadcast_in_dim.17), calls=%async_computation | async-start | bytes 3145728 | tf_op jit(solution)/shard_map/all_to_all | solution.py:32
  161.4 1.9 copy.59
  163.3 18.7 %all-to-all-done = bf16[8,768,128]{1,2,0:T(8,128)(2,1)S(1)} async-done(((bf16[8,768,128]{1,2,0:T(8,128)(2,1)}), bf16[8,768,128]{1,2,0:T(8,128)(2,1)S(1)}, u32[]{:S(2)}, u32[]{:S(2)}) %all-to-all-start) | async-done | bytes 1572896 | tf_op jit(solution)/shard_map/all_to_all | solution.py:32
  182.0 0.2 fusion.35
  182.2 0.2 fusion.34
  182.5 0.2 fusion.32
  182.7 0.2 fusion.30
  183.0 0.2 fusion.28
  183.2 0.2 fusion.26
  183.5 0.2 fusion.24
  184.0 0.3 multiply_reduce_fusion.1
  184.3 0.6 broadcast_in_dim.18
  184.9 4.2 %all-to-all-start.2 = ((f32[8,1,768]{2,1,0:T(1,128)}), f32[8,1,768]{2,1,0:T(1,128)S(1)}, u32[]{:S(2)}, u32[]{:S(2)}) async-start(f32[8,1,768]{2,1,0:T(1,128)} %broadcast_in_dim.18), calls=%async_computation.2 | async-start | bytes 49152 | tf_op jit(solution)/shard_map/all_to_all | solution.py:32
  189.1 0.8 dynamic_slice.25
  189.9 3.9 %all-to-all-done.2 = f32[8,1,768]{2,1,0:T(1,128)S(1)} async-done(((f32[8,1,768]{2,1,0:T(1,128)}), f32[8,1,768]{2,1,0:T(1,128)S(1)}, u32[]{:S(2)}, u32[]{:S(2)}) %all-to-all-start.2) | async-done | bytes 24608 | tf_op jit(solution)/shard_map/all_to_all | solution.py:32
  193.9 0.9 multiply_convert_fusion.1
  195.0 0.3 all-gather.11.cloned.1.call-update
  195.3 24.9 %all-gather.7.cloned.1.call-done = bf16[768,2048]{0,1:T(8,128)(2,1)} async-done(((bf16[768,256]{0,1:T(8,128)(2,1)}), bf16[768,2048]{0,1:T(8,128)(2,1)}) %all-gather.7.cloned.1.call-update) | async-done | bytes 3145744 | tf_op jit(solution)/shard_map/all_gather | solution.py:168
  220.2 5.2 %fusion.16 = f32[768,704]{0,1:T(8,128)S(1)} fusion(bf16[768,2048]{0,1:T(8,128)(2,1)} %all-gather.7.cloned.1.call-done, bf16[2048,1408]{0,1:T(8,128)(2,1)} %all-gather.9.cloned.1.call-done), kind=kOutput, calls=%fused_computation.22 | convolution fusion | flops 2214592512 | bytes 8192000 | tf_op jit(solution)/shard_map/dot_general | solution.py:170
  225.4 45.8 %all-gather.11.cloned.1.call-done = bf16[704,2048]{1,0:T(8,128)(2,1)} async-done(((bf16[704,128]{1,0:T(8,128)(2,1)}), bf16[704,2048]{1,0:T(8,128)(2,1)}) %all-gather.11.cloned.1.call-update) | async-done | bytes 2883600 | tf_op jit(solution)/shard_map/all_gather | solution.py:175
  271.2 11.7 %convolution_convert_fusion = bf16[768,2048]{1,0:T(8,128)(2,1)} fusion(bf16[704,2048]{1,0:T(8,128)(2,1)} %all-gather.11.cloned.1.call-done, f32[768,704]{0,1:T(8,128)S(1)} %fusion.16, bf16[768,2048]{0,1:T(8,128)(2,1)} %all-gather.7.cloned.1.call-done, bf16[2048,1408]{0,1:T(8,128)(2,1)} %all-gather.9.cloned.1.call-done), kind=kOutput, calls=%fused_computation.18 | convolution fusion | flops 4434001920 | bytes 14221312 | tf_op jit(solution)/shard_map/dot_general | solution.py:173
  282.9 2.1 copy.79
  285.0 43.5 %all_to_all.32 = bf16[8,768,256]{2,1,0:T(8,128)(2,1)S(1)} all-to-all(bf16[8,768,256]{2,1,0:T(8,128)(2,1)S(1)} %bitcast.66), channel_id=1, replica_groups=mesh['sp'=16,'tp'=8] {'tp'}, dimensions={0} | all-to-all | bytes 6291456 | tf_op jit(solution)/shard_map/all_to_all | solution.py:52
  328.5 0.4 convert_reduce_fusion
  329.0 0.3 copy.73
  329.3 0.9 copy.74
  (58 shorter events, 1.4 us)
Async XLA Ops:
  6.5 2.4 copy-start
  6.5 71.7 %all-gather.5.cloned.1.call-start = ((), (), s32[]{:S(2)}) async-start(), calls=%async_computation.4 | async-start | bytes 6684672 | tf_op jit(solution)/shard_map/all_gather | solution.py:21
  10.5 3.1 copy-start.3
  12.3 8.1 %copy-start.4 = (bf16[128,704]{0,1:T(8,128)(2,1)S(1)}, bf16[128,704]{0,1:T(8,128)(2,1)}, u32[]{:S(2)}) copy-start(bf16[128,704]{0,1:T(8,128)(2,1)} %param.22) | copy-start | bytes 540676
  12.3 8.1 %copy-start.5 = (bf16[128,704]{0,1:T(8,128)(2,1)S(1)}, bf16[128,704]{0,1:T(8,128)(2,1)}, u32[]{:S(2)}) copy-start(bf16[128,704]{0,1:T(8,128)(2,1)} %param.21) | copy-start | bytes 540676
  14.6 140.2 %all-to-all-start.1 = ((bf16[128,8,256]{0,2,1:T(8,128)(2,1)}), bf16[128,8,256]{0,2,1:T(8,128)(2,1)S(1)}, u32[]{:S(2)}, u32[]{:S(2)}) async-start(bf16[128,8,256]{0,2,1:T(8,128)(2,1)} %bitcast.9), calls=%async_computation.1 | async-start | bytes 1048576 | tf_op jit(solution)/shard_map/all_to_all | solution.py:100
  20.4 174.9 %all-gather.9.cloned.1.call-start = ((), (), s32[]{:S(2)}) async-start(), calls=%async_computation.6 | async-start | bytes 6127616 | tf_op jit(solution)/shard_map/all_gather | solution.py:21
  87.6 5.0 %copy-start.1 = (f32[2048,768]{1,0:T(8,128)S(1)}, f32[2048,768]{1,0:T(8,128)}, u32[]{:S(2)}) copy-start(f32[2048,768]{1,0:T(8,128)} %get-tuple-element.238) | copy-start | bytes 18874372 | tf_op jit(solution)/shard_map/while
  99.6 4.7 %copy-start.1 = (f32[2048,768]{1,0:T(8,128)S(1)}, f32[2048,768]{1,0:T(8,128)}, u32[]{:S(2)}) copy-start(f32[2048,768]{1,0:T(8,128)} %get-tuple-element.238) | copy-start | bytes 18874372 | tf_op jit(solution)/shard_map/while
  111.4 5.0 %copy-start.1 = (f32[2048,768]{1,0:T(8,128)S(1)}, f32[2048,768]{1,0:T(8,128)}, u32[]{:S(2)}) copy-start(f32[2048,768]{1,0:T(8,128)} %get-tuple-element.238) | copy-start | bytes 18874372 | tf_op jit(solution)/shard_map/while
  123.5 5.0 %copy-start.1 = (f32[2048,768]{1,0:T(8,128)S(1)}, f32[2048,768]{1,0:T(8,128)}, u32[]{:S(2)}) copy-start(f32[2048,768]{1,0:T(8,128)} %get-tuple-element.238) | copy-start | bytes 18874372 | tf_op jit(solution)/shard_map/while
  135.6 4.9 %copy-start.1 = (f32[2048,768]{1,0:T(8,128)S(1)}, f32[2048,768]{1,0:T(8,128)}, u32[]{:S(2)}) copy-start(f32[2048,768]{1,0:T(8,128)} %get-tuple-element.238) | copy-start | bytes 18874372 | tf_op jit(solution)/shard_map/while
  147.5 4.6 %copy-start.1 = (f32[2048,768]{1,0:T(8,128)S(1)}, f32[2048,768]{1,0:T(8,128)}, u32[]{:S(2)}) copy-start(f32[2048,768]{1,0:T(8,128)} %get-tuple-element.238) | copy-start | bytes 18874372 | tf_op jit(solution)/shard_map/while
  156.2 25.8 %all-to-all-start = ((bf16[8,768,128]{1,2,0:T(8,128)(2,1)}), bf16[8,768,128]{1,2,0:T(8,128)(2,1)S(1)}, u32[]{:S(2)}, u32[]{:S(2)}) async-start(bf16[8,768,128]{1,2,0:T(8,128)(2,1)} %broadcast_in_dim.17), calls=%async_computation | async-start | bytes 3145728 | tf_op jit(solution)/shard_map/all_to_all | solution.py:32
  183.0 1.0 copy-start.2
  184.9 8.9 %all-to-all-start.2 = ((f32[8,1,768]{2,1,0:T(1,128)}), f32[8,1,768]{2,1,0:T(1,128)S(1)}, u32[]{:S(2)}, u32[]{:S(2)}) async-start(f32[8,1,768]{2,1,0:T(1,128)} %broadcast_in_dim.18), calls=%async_computation.2 | async-start | bytes 49152 | tf_op jit(solution)/shard_map/all_to_all | solution.py:32
  189.1 31.1 %all-gather.7.cloned.1.call-start = ((), (), s32[]{:S(2)}) async-start(), calls=%async_computation.5 | async-start | bytes 3538944 | tf_op jit(solution)/shard_map/all_gather | solution.py:168
  194.7 76.4 %all-gather.11.cloned.1.call-start = ((), (), s32[]{:S(2)}) async-start(), calls=%async_computation.7 | async-start | bytes 3063808 | tf_op jit(solution)/shard_map/all_gather | solution.py:175
Sparse Core Ops, SparseCore 0:
  13.7 64.4 all-gather.4
  80.3 62.8 all-gather.8
  194.9 25.3 all-gather.6
  222.2 48.9 all-gather.10
where the time goes:
time: 338 us; the launch traced here: 337 us
  waiting for transfers between devices  151 us (45%)
  matrix products  61.1 us (18%)
  blocking collectives  43.5 us (13%)
  other arithmetic  34.3 us (10%)
  local copies, waits for them, and re-layouts  18.2 us (5%)
  starting transfers between devices  15.5 us (5%)
  between operations  13.4 us (4%)
    all_gather x2, waiting for transfers between devices, sent_together(): lax.all_gather(both, axis, axis=dim, tiled=True)  56.8 us
    all_gather x1, waiting for transfers between devices, on_device(): lax.all_gather(down_weight, 'sp', axis=1, tiled=True)  45.8 us
    all_to_all x1, blocking collectives, summed_on_arrival(): lax.all_to_all(tiles, axis, split_axis=0, concat_axis=0, tiled=True)  43.5 us
    dot_general x6, matrix products, one_block(): jnp.dot(query_matrix, block_keys.T, preferred_element_type=jnp.float32)  28 us
    all_gather x1, waiting for transfers between devices, on_device(): normed = lax.all_gather(normed_own, 'tp', axis=1, tiled=True)  24.9 us
    reduce_sum x6, other arithmetic, one_block(): running_sum = running_sum * factor + jnp.sum(weights, axis=1)  24.8 us
    all_to_all x2, waiting for transfers between devices, sent_to_all(): lax.all_to_all(jnp.broadcast_to(x[None], (size, *x.shape)), axis, 0, 0, t...  22.6 us
    dot_general x6, matrix products, one_block(): jnp.dot(weights.astype(jnp.bfloat16), block_values, preferred_element_typ...  14.2 us
  transfers between devices with their start and end apart: 7, of which 5 were waited for; matrix products, arithmetic and copies ran while one was open for 26% of the time, Pallas kernels for 0%

commit v1 on v0

--- a/solution.py
+++ b/solution.py
@@ -172,7 +172,7 @@
     hidden = (jax.nn.silu(gate_out) * up_out).astype(jnp.bfloat16)
     down_terms = jnp.dot(
         hidden,
-        lax.all_gather(down_weight, "sp", axis=1, tiled=True),
+        jnp.concatenate(lax.all_gather(down_weight, "sp"), axis=1),
         preferred_element_type=jnp.float32,
     )
     down_share = summed_on_arrival(down_terms.astype(jnp.bfloat16), "tp", 1)

time: 338 us -> 291 us (0.86)
  waiting for transfers between devices: 151 us -> 102 us
  local copies, waits for them, and re-layouts: 18.2 us -> 23.1 us
    all_gather x1, waiting for transfers between devices: 45.8 us -> 0.02 us  [on_device(): lax.all_gather(down_weight, 'sp')]
    all_gather x0 -> x1, local copies, waits for them, and re-layouts: none -> 5.27 us  [on_device(): lax.all_gather(down_weight, 'sp')]
  transfers between devices with their start and end apart: 7 -> 7, of which waited for: 5 -> 4; matrix products, arithmetic and copies ran while one was open for 26% -> 30% of each run, Pallas kernels for 0% -> 0%
where the time goes in v1:
time: 291 us; the launch traced here: 289 us
  waiting for transfers between devices  102 us (35%)
  matrix products  61.3 us (21%)
  blocking collectives  40.4 us (14%)
  other arithmetic  33.7 us (12%)
  local copies, waits for them, and re-layouts  23.1 us (8%)
  starting transfers between devices  15.2 us (5%)
  between operations  13.4 us (5%)
    all_gather x2, waiting for transfers between devices, sent_together(): lax.all_gather(both, axis, axis=dim, tiled=True)  56.1 us
    all_to_all x1, blocking collectives, summed_on_arrival(): lax.all_to_all(tiles, axis, split_axis=0, concat_axis=0, tiled=True)  40.4 us
    dot_general x6, matrix products, one_block(): jnp.dot(query_matrix, block_keys.T, preferred_element_type=jnp.float32)  28 us
    reduce_sum x6, other arithmetic, one_block(): running_sum = running_sum * factor + jnp.sum(weights, axis=1)  24.3 us
    all_to_all x2, waiting for transfers between devices, sent_to_all(): lax.all_to_all(jnp.broadcast_to(x[None], (size, *x.shape)), axis, 0, 0, t...  22.7 us
    all_gather x1, waiting for transfers between devices, on_device(): normed = lax.all_gather(normed_own, 'tp', axis=1, tiled=True)  22.6 us
    dot_general x6, matrix products, one_block(): jnp.dot(weights.astype(jnp.bfloat16), block_values, preferred_element_typ...  14.3 us
    dot_general x1, matrix products, on_device(): jnp.dot(hidden, jnp.concatenate(lax.all_gather(down_weight, 'sp'), axis=1...  11.8 us
  transfers between devices with their start and end apart: 7, of which 4 were waited for; matrix products, arithmetic and copies ran while one was open for 30% of the time, Pallas kernels for 0%

profile of v1, /device:TPU:1, one launch (start us, length us, event | category | flops | bytes accessed | tf_op | source)
XLA Modules:
  0.0 289.5 jit_solution(3912065818291232085)
XLA Ops:
  6.6 1.1 fusion.40
  7.7 1.1 fusion.43
  8.9 0.3 multiply_bitcast_fusion.1
  9.2 1.3 fusion.42
  10.5 1.8 fusion.46
  12.3 0.3 subtract_convert_fusion.1
  12.8 0.8 pad_maximum_fusion.1
  13.7 0.7 all-gather.12.cloned.1.call-update
  14.4 1.0 copy.65
  15.4 5.8 %all-to-all-start.1 = ((bf16[128,8,256]{0,2,1:T(8,128)(2,1)}), bf16[128,8,256]{0,2,1:T(8,128)(2,1)S(1)}, u32[]{:S(2)}, u32[]{:S(2)}) async-start(bf16[128,8,256]{0,2,1:T(8,128)(2,1)} %bitcast.9), calls=%async_computation.1 | async-start | bytes 1048576 | tf_op jit(solution)/shard_map/all_to_all | solution.py:100
  21.2 0.8 pad_maximum_fusion.2
  22.2 56.0 %all-gather.6.cloned.1.call-done = bf16[12288,256]{1,0:T(8,128)(2,1)} async-done(((bf16[768,256]{1,0:T(8,128)(2,1)}), bf16[12288,256]{1,0:T(8,128)(2,1)}) %all-gather.6.cloned.1.call-update) | async-done | bytes 6291472 | tf_op jit(solution)/shard_map/all_gather | solution.py:21
  78.2 4.7 %fusion.68 = (bf16[12288,128]{1,0:T(8,128)(2,1)}, bf16[12288,128]{1,0:T(8,128)(2,1)}) fusion(bf16[12288,256]{1,0:T(8,128)(2,1)} %all-gather.6.cloned.1.call-done), kind=kLoop, calls=%fused_computation.116 | loop fusion | bytes 12582912 | tf_op jit(solution)/shard_map/split | solution.py:21
  82.9 70.7 %while.18 = (s32[]{:T(128)}, f32[768]{0:T(1024)S(1)}, f32[768]{0:T(1024)S(1)}, f32[768,128]{1,0:T(8,128)S(1)}, bf16[12288,128]{1,0:T(8,128)(2,1)}, /*index=5*/bf...) while((s32[]{:T(128)}, f32[768]{0:T(1024)S(1)}, ...), condition=%wide.region_5.6_spmd.clone, body=%wide.region_2.5_spmd.clone.sunk | while | flops 818188032 | bytes 46121160 | solution.py:146
  82.9 4.7 %multiply_reduce_fusion.3 = (f32[768]{0:T(1024)S(1)}, f32[2048,768]{1,0:T(8,128)}) fusion(bf16[768,128]{1,0:T(8,128)(2,1)S(1)} %get-tuple-element.268, bf16[12288,128]{1,0:T(8,128)(2,1)} %get-tuple-element.267, s32[]{:T(128)S(6)} %select_n.55), kind=kOutput, calls=%fused_computation.1.clone.1 | convolution fusion | flops 405798144 | bytes 7015428 | tf_op jit(solution)/shard_map/while/body/eval_jaxpr/dot_general | solution.py:135
  87.6 4.1 %fusion.81 = f32[768]{0:T(1024)S(1)} fusion(f32[2048,768]{1,0:T(8,128)} %get-tuple-element.238, f32[768]{0:T(1024)S(1)} %select_maximum_fusion.2), kind=kLoop, calls=%fused_computation.3.clone.1 | loop fusion | flops 4717824 | bytes 6297600 | tf_op jit(solution)/shard_map/while/body/eval_jaxpr/reduce_sum | solution.py:140
  91.7 0.7 copy-done.1
  92.4 2.4 fusion.83
  94.8 4.7 %multiply_reduce_fusion.3 = (f32[768]{0:T(1024)S(1)}, f32[2048,768]{1,0:T(8,128)}) fusion(bf16[768,128]{1,0:T(8,128)(2,1)S(1)} %get-tuple-element.268, bf16[12288,128]{1,0:T(8,128)(2,1)} %get-tuple-element.267, s32[]{:T(128)S(6)} %select_n.55), kind=kOutput, calls=%fused_computation.1.clone.1 | convolution fusion | flops 405798144 | bytes 7015428 | tf_op jit(solution)/shard_map/while/body/eval_jaxpr/dot_general | solution.py:135
  99.5 4.0 %fusion.81 = f32[768]{0:T(1024)S(1)} fusion(f32[2048,768]{1,0:T(8,128)} %get-tuple-element.238, f32[768]{0:T(1024)S(1)} %select_maximum_fusion.2), kind=kLoop, calls=%fused_computation.3.clone.1 | loop fusion | flops 4717824 | bytes 6297600 | tf_op jit(solution)/shard_map/while/body/eval_jaxpr/reduce_sum | solution.py:140
  103.5 0.6 copy-done.1
  104.1 2.4 fusion.83
  106.5 4.7 %multiply_reduce_fusion.3 = (f32[768]{0:T(1024)S(1)}, f32[2048,768]{1,0:T(8,128)}) fusion(bf16[768,128]{1,0:T(8,128)(2,1)S(1)} %get-tuple-element.268, bf16[12288,128]{1,0:T(8,128)(2,1)} %get-tuple-element.267, s32[]{:T(128)S(6)} %select_n.55), kind=kOutput, calls=%fused_computation.1.clone.1 | convolution fusion | flops 405798144 | bytes 7015428 | tf_op jit(solution)/shard_map/while/body/eval_jaxpr/dot_general | solution.py:135
  111.2 4.0 %fusion.81 = f32[768]{0:T(1024)S(1)} fusion(f32[2048,768]{1,0:T(8,128)} %get-tuple-element.238, f32[768]{0:T(1024)S(1)} %select_maximum_fusion.2), kind=kLoop, calls=%fused_computation.3.clone.1 | loop fusion | flops 4717824 | bytes 6297600 | tf_op jit(solution)/shard_map/while/body/eval_jaxpr/reduce_sum | solution.py:140
  115.2 0.6 copy-done.1
  115.8 2.4 fusion.83
  118.2 4.7 %multiply_reduce_fusion.3 = (f32[768]{0:T(1024)S(1)}, f32[2048,768]{1,0:T(8,128)}) fusion(bf16[768,128]{1,0:T(8,128)(2,1)S(1)} %get-tuple-element.268, bf16[12288,128]{1,0:T(8,128)(2,1)} %get-tuple-element.267, s32[]{:T(128)S(6)} %select_n.55), kind=kOutput, calls=%fused_computation.1.clone.1 | convolution fusion | flops 405798144 | bytes 7015428 | tf_op jit(solution)/shard_map/while/body/eval_jaxpr/dot_general | solution.py:135
  122.9 4.0 %fusion.81 = f32[768]{0:T(1024)S(1)} fusion(f32[2048,768]{1,0:T(8,128)} %get-tuple-element.238, f32[768]{0:T(1024)S(1)} %select_maximum_fusion.2), kind=kLoop, calls=%fused_computation.3.clone.1 | loop fusion | flops 4717824 | bytes 6297600 | tf_op jit(solution)/shard_map/while/body/eval_jaxpr/reduce_sum | solution.py:140
  126.9 0.6 copy-done.1
  127.5 2.4 fusion.83
  129.9 4.7 %multiply_reduce_fusion.3 = (f32[768]{0:T(1024)S(1)}, f32[2048,768]{1,0:T(8,128)}) fusion(bf16[768,128]{1,0:T(8,128)(2,1)S(1)} %get-tuple-element.268, bf16[12288,128]{1,0:T(8,128)(2,1)} %get-tuple-element.267, s32[]{:T(128)S(6)} %select_n.55), kind=kOutput, calls=%fused_computation.1.clone.1 | convolution fusion | flops 405798144 | bytes 7015428 | tf_op jit(solution)/shard_map/while/body/eval_jaxpr/dot_general | solution.py:135
  134.6 4.0 %fusion.81 = f32[768]{0:T(1024)S(1)} fusion(f32[2048,768]{1,0:T(8,128)} %get-tuple-element.238, f32[768]{0:T(1024)S(1)} %select_maximum_fusion.2), kind=kLoop, calls=%fused_computation.3.clone.1 | loop fusion | flops 4717824 | bytes 6297600 | tf_op jit(solution)/shard_map/while/body/eval_jaxpr/reduce_sum | solution.py:140
  138.6 0.8 copy-done.1
  139.4 2.4 fusion.83
  141.8 4.7 %multiply_reduce_fusion.3 = (f32[768]{0:T(1024)S(1)}, f32[2048,768]{1,0:T(8,128)}) fusion(bf16[768,128]{1,0:T(8,128)(2,1)S(1)} %get-tuple-element.268, bf16[12288,128]{1,0:T(8,128)(2,1)} %get-tuple-element.267, s32[]{:T(128)S(6)} %select_n.55), kind=kOutput, calls=%fused_computation.1.clone.1 | convolution fusion | flops 405798144 | bytes 7015428 | tf_op jit(solution)/shard_map/while/body/eval_jaxpr/dot_general | solution.py:135
  146.5 4.1 %fusion.81 = f32[768]{0:T(1024)S(1)} fusion(f32[2048,768]{1,0:T(8,128)} %get-tuple-element.238, f32[768]{0:T(1024)S(1)} %select_maximum_fusion.2), kind=kLoop, calls=%fused_computation.3.clone.1 | loop fusion | flops 4717824 | bytes 6297600 | tf_op jit(solution)/shard_map/while/body/eval_jaxpr/reduce_sum | solution.py:140
  150.6 0.6 copy-done.1
  151.2 2.4 fusion.83
  153.9 1.3 broadcast_in_dim.17
  155.2 5.1 %all-to-all-start = ((bf16[8,768,128]{1,2,0:T(8,128)(2,1)}), bf16[8,768,128]{1,2,0:T(8,128)(2,1)S(1)}, u32[]{:S(2)}, u32[]{:S(2)}) async-start(bf16[8,768,128]{1,2,0:T(8,128)(2,1)} %broadcast_in_dim.17), calls=%async_computation | async-start | bytes 3145728 | tf_op jit(solution)/shard_map/all_to_all | solution.py:32
  160.4 1.9 copy.63
  162.3 18.7 %all-to-all-done = bf16[8,768,128]{1,2,0:T(8,128)(2,1)S(1)} async-done(((bf16[8,768,128]{1,2,0:T(8,128)(2,1)}), bf16[8,768,128]{1,2,0:T(8,128)(2,1)S(1)}, u32[]{:S(2)}, u32[]{:S(2)}) %all-to-all-start) | async-done | bytes 1572896 | tf_op jit(solution)/shard_map/all_to_all | solution.py:32
  180.9 0.2 fusion.37
  181.2 0.2 fusion.36
  181.4 0.2 fusion.34
  181.7 0.2 fusion.32
  182.0 0.2 fusion.30
  182.2 0.2 fusion.28
  182.5 0.2 fusion.26
  182.9 0.3 multiply_reduce_fusion.1
  183.2 0.6 broadcast_in_dim.18
  183.9 4.2 %all-to-all-start.2 = ((f32[8,1,768]{2,1,0:T(1,128)}), f32[8,1,768]{2,1,0:T(1,128)S(1)}, u32[]{:S(2)}, u32[]{:S(2)}) async-start(f32[8,1,768]{2,1,0:T(1,128)} %broadcast_in_dim.18), calls=%async_computation.2 | async-start | bytes 49152 | tf_op jit(solution)/shard_map/all_to_all | solution.py:32
  188.1 0.8 dynamic_slice.25
  188.8 4.0 %all-to-all-done.2 = f32[8,1,768]{2,1,0:T(1,128)S(1)} async-done(((f32[8,1,768]{2,1,0:T(1,128)}), f32[8,1,768]{2,1,0:T(1,128)S(1)}, u32[]{:S(2)}, u32[]{:S(2)}) %all-to-all-start.2) | async-done | bytes 24608 | tf_op jit(solution)/shard_map/all_to_all | solution.py:32
  192.9 0.9 multiply_convert_fusion.1
  193.8 5.3 %copy.75 = bf16[16,704,128]{2,0,1:T(8,128)(2,1)} copy(bf16[16,704,128]{2,1,0:T(8,128)(2,1)} %bitcast.81) | data formatting | bytes 5767168 | tf_op jit(solution)/shard_map/all_gather | solution.py:175
  199.1 22.6 %all-gather.8.cloned.1.call-done = bf16[768,2048]{0,1:T(8,128)(2,1)} async-done(((bf16[768,256]{0,1:T(8,128)(2,1)}), bf16[768,2048]{0,1:T(8,128)(2,1)}) %all-gather.8.cloned.1.call-update) | async-done | bytes 3145744 | tf_op jit(solution)/shard_map/all_gather | solution.py:168
  221.7 5.2 %fusion.18 = f32[768,704]{0,1:T(8,128)S(1)} fusion(bf16[768,2048]{0,1:T(8,128)(2,1)} %all-gather.8.cloned.1.call-done, bf16[2048,1408]{0,1:T(8,128)(2,1)} %all-gather.10.cloned.1.call-done), kind=kOutput, calls=%fused_computation.24 | convolution fusion | flops 2214592512 | bytes 8192000 | tf_op jit(solution)/shard_map/dot_general | solution.py:170
  226.9 11.8 %convolution_convert_fusion = bf16[768,2048]{1,0:T(8,128)(2,1)} fusion(bf16[88,8,16,128]{3,2,1,0:T(8,128)(2,1)} %bitcast.82, f32[768,704]{0,1:T(8,128)S(1)} %fusion.18, bf16[768,2048]{0,1:T(8,128)(2,1)} %all-gather.8.cloned.1.call-done, bf16[2048,1408]{0,1:T(8,128)(2,1)} %all-gather.10.cloned.1.call-done), kind=kOutput, calls=%fused_computation.18 | convolution fusion | flops 4434001920 | bytes 14221312 | tf_op jit(solution)/shard_map/dot_general | solution.py:173
  238.7 2.1 copy.89
  240.8 40.4 %all_to_all.32 = bf16[8,768,256]{2,1,0:T(8,128)(2,1)S(1)} all-to-all(bf16[8,768,256]{2,1,0:T(8,128)(2,1)S(1)} %bitcast.71), channel_id=1, replica_groups=mesh['sp'=16,'tp'=8] {'tp'}, dimensions={0} | all-to-all | bytes 6291456 | tf_op jit(solution)/shard_map/all_to_all | solution.py:52
  281.2 0.4 convert_reduce_fusion
  281.6 0.3 copy.78
  282.0 0.9 copy.79
  (59 shorter events, 1.3 us)
Async XLA Ops:
  6.5 2.4 copy-start
  6.5 71.7 %all-gather.6.cloned.1.call-start = ((), (), s32[]{:S(2)}) async-start(), calls=%async_computation.4 | async-start | bytes 6684672 | tf_op jit(solution)/shard_map/all_gather | solution.py:21
  10.5 3.8 %copy-start.3 = (bf16[128,2048]{1,0:T(8,128)(2,1)S(1)}, bf16[128,2048]{1,0:T(8,128)(2,1)}, u32[]{:S(2)}) copy-start(bf16[128,2048]{1,0:T(8,128)(2,1)} %param.19) | copy-start | bytes 1572868
  12.3 8.9 %copy-start.4 = (bf16[128,704]{0,1:T(8,128)(2,1)S(1)}, bf16[128,704]{0,1:T(8,128)(2,1)}, u32[]{:S(2)}) copy-start(bf16[128,704]{0,1:T(8,128)(2,1)} %param.22) | copy-start | bytes 540676
  12.3 8.9 %copy-start.5 = (bf16[128,704]{0,1:T(8,128)(2,1)S(1)}, bf16[128,704]{0,1:T(8,128)(2,1)}, u32[]{:S(2)}) copy-start(bf16[128,704]{0,1:T(8,128)(2,1)} %param.21) | copy-start | bytes 540676
  13.6 180.2 %all-gather.12.cloned.1.call-start = ((), (), s32[]{:S(2)}) async-start(), calls=%async_computation.7 | async-start | bytes 3063808 | tf_op jit(solution)/shard_map/all_gather | solution.py:175
  15.4 138.5 %all-to-all-start.1 = ((bf16[128,8,256]{0,2,1:T(8,128)(2,1)}), bf16[128,8,256]{0,2,1:T(8,128)(2,1)S(1)}, u32[]{:S(2)}, u32[]{:S(2)}) async-start(bf16[128,8,256]{0,2,1:T(8,128)(2,1)} %bitcast.9), calls=%async_computation.1 | async-start | bytes 1048576 | tf_op jit(solution)/shard_map/all_to_all | solution.py:100
  21.2 177.9 %all-gather.10.cloned.1.call-start = ((), (), s32[]{:S(2)}) async-start(), calls=%async_computation.6 | async-start | bytes 6127616 | tf_op jit(solution)/shard_map/all_gather | solution.py:21
  87.6 4.8 %copy-start.1 = (f32[2048,768]{1,0:T(8,128)S(1)}, f32[2048,768]{1,0:T(8,128)}, u32[]{:S(2)}) copy-start(f32[2048,768]{1,0:T(8,128)} %get-tuple-element.238) | copy-start | bytes 18874372 | tf_op jit(solution)/shard_map/while
  99.5 4.6 %copy-start.1 = (f32[2048,768]{1,0:T(8,128)S(1)}, f32[2048,768]{1,0:T(8,128)}, u32[]{:S(2)}) copy-start(f32[2048,768]{1,0:T(8,128)} %get-tuple-element.238) | copy-start | bytes 18874372 | tf_op jit(solution)/shard_map/while
  111.2 4.6 %copy-start.1 = (f32[2048,768]{1,0:T(8,128)S(1)}, f32[2048,768]{1,0:T(8,128)}, u32[]{:S(2)}) copy-start(f32[2048,768]{1,0:T(8,128)} %get-tuple-element.238) | copy-start | bytes 18874372 | tf_op jit(solution)/shard_map/while
  122.9 4.6 %copy-start.1 = (f32[2048,768]{1,0:T(8,128)S(1)}, f32[2048,768]{1,0:T(8,128)}, u32[]{:S(2)}) copy-start(f32[2048,768]{1,0:T(8,128)} %get-tuple-element.238) | copy-start | bytes 18874372 | tf_op jit(solution)/shard_map/while
  134.6 4.8 %copy-start.1 = (f32[2048,768]{1,0:T(8,128)S(1)}, f32[2048,768]{1,0:T(8,128)}, u32[]{:S(2)}) copy-start(f32[2048,768]{1,0:T(8,128)} %get-tuple-element.238) | copy-start | bytes 18874372 | tf_op jit(solution)/shard_map/while
  146.5 4.7 %copy-start.1 = (f32[2048,768]{1,0:T(8,128)S(1)}, f32[2048,768]{1,0:T(8,128)}, u32[]{:S(2)}) copy-start(f32[2048,768]{1,0:T(8,128)} %get-tuple-element.238) | copy-start | bytes 18874372 | tf_op jit(solution)/shard_map/while
  155.2 25.7 %all-to-all-start = ((bf16[8,768,128]{1,2,0:T(8,128)(2,1)}), bf16[8,768,128]{1,2,0:T(8,128)(2,1)S(1)}, u32[]{:S(2)}, u32[]{:S(2)}) async-start(bf16[8,768,128]{1,2,0:T(8,128)(2,1)} %broadcast_in_dim.17), calls=%async_computation | async-start | bytes 3145728 | tf_op jit(solution)/shard_map/all_to_all | solution.py:32
  181.9 1.0 copy-start.2
  183.9 9.0 %all-to-all-start.2 = ((f32[8,1,768]{2,1,0:T(1,128)}), f32[8,1,768]{2,1,0:T(1,128)S(1)}, u32[]{:S(2)}, u32[]{:S(2)}) async-start(f32[8,1,768]{2,1,0:T(1,128)} %broadcast_in_dim.18), calls=%async_computation.2 | async-start | bytes 49152 | tf_op jit(solution)/shard_map/all_to_all | solution.py:32
  188.1 33.6 %all-gather.8.cloned.1.call-start = ((), (), s32[]{:S(2)}) async-start(), calls=%async_computation.5 | async-start | bytes 3538944 | tf_op jit(solution)/shard_map/all_gather | solution.py:168
Sparse Core Ops, SparseCore 0:
  13.7 64.4 all-gather.5
  80.3 46.0 all-gather.11
  128.6 62.8 all-gather.9
  193.9 27.7 all-gather.7
